TPU v7x, 32 devices: a whole 2x2x4 slice. The times are simulated.
32 devices in a mesh: sp: 4 (over y, core), tp: 8 (over z, x).
Axes of the slice: x: 2, y: 2, z: 4, core: 2. Of those that a mesh axis runs over, the one named last changes fastest.
Arguments:
- latent: bfloat16 [960, 2048], P(('sp', 'tp')), may hold values from -40 to 40
- context: bfloat16 [768, 2048], P('sp'), may hold values from -6 to 6
- cond_latent: float32 [2048], P('sp'), may hold values from -6 to 6
- cond_context: float32 [2048], P('sp'), may hold values from -6 to 6
- mod_weight: bfloat16 [2048, 6144], P('sp', 'tp'), may hold values from -0.125 to 0.125
- w_query: bfloat16 [2048, 1024], P(None, 'tp'), may hold values from -5 to 5
- w_key: bfloat16 [2048, 1024], P(None, 'tp'), may hold values from -5 to 5
- w_value: bfloat16 [2048, 1024], P(None, 'tp'), may hold values from -0.125 to 0.125
- w_out: bfloat16 [1024, 2048], P('tp'), may hold values from -0.1875 to 0.1875
- head_lambda: float32 [8], P('tp'), may hold values from 0.3 to 0.8
Outputs:
- mixed_latent: bfloat16 [960, 2048], P(('sp', 'tp'))
All inputs are finite; a program needn't handle non-finite values.
Results may differ from a plain program's by a relative error of at most 0.011.
Values may be sent and summed in bfloat16 or wider, within the bound.
A program may use at most 64 MiB of HBM per device.

v0:
```python
import jax
import jax.numpy as jnp
from jax import lax
from jax.sharding import PartitionSpec as P

QK_DIM = 64
VAL_DIM = 128
GRID_W = 64
NORM_EPS = 0.01
HEAD_EPS = 0.001
THETA = 10000.0


def modulate_rows(rows, shift, scale):
    values = rows.astype(jnp.float32)
    normed = values * lax.rsqrt(jnp.mean(values * values, axis=-1, keepdims=True) + NORM_EPS)
    return (normed * (1.0 + scale) + shift).astype(jnp.bfloat16)


def rotary_tables(positions):
    quarter = QK_DIM // 4
    inverse = THETA ** (-jnp.arange(quarter, dtype=jnp.float32) / quarter)
    grid_row = (positions // GRID_W).astype(jnp.float32)
    grid_column = (positions % GRID_W).astype(jnp.float32)
    by_row = grid_row[:, None] * inverse[None, :]
    by_column = grid_column[:, None] * inverse[None, :]
    angle = jnp.concatenate([by_row, by_row, by_column, by_column], axis=-1)
    return (jnp.cos(angle), jnp.sin(angle))


def rotate(product, cosine, sine):
    number = product.shape[0]
    quarter = QK_DIM // 4
    half = QK_DIM // 2
    shaped = product.reshape(number, -1, QK_DIM)
    first = shaped[..., :half]
    second = shaped[..., half:]
    turned = jnp.concatenate(
        [
            -first[..., quarter:],
            first[..., :quarter],
            -second[..., quarter:],
            second[..., :quarter],
        ],
        axis=-1,
    )
    result = shaped * cosine[:, None, :] + turned * sine[:, None, :]
    return result.reshape(number, -1).astype(jnp.bfloat16)


def attend_piece(state, piece, queries):
    highest, totals, carried = state
    keys, values = piece
    number = keys.shape[0]
    heads = queries.shape[1]
    key_heads = keys.reshape(number, heads, 2, QK_DIM)
    value_heads = values.reshape(number, heads, VAL_DIM)
    scores = jnp.einsum(
        "qhmd,khmd->hmqk", queries, key_heads, preferred_element_type=jnp.float32
    ) * QK_DIM ** (-0.5)
    new_highest = jnp.maximum(highest, jnp.max(scores, axis=-1))
    weights = jnp.exp(scores - new_highest[..., None])
    totals = jnp.sum(weights, axis=-1)
    mixed = jnp.einsum(
        "hmqk,khd->hmqd",
        weights.astype(jnp.bfloat16),
        value_heads,
        preferred_element_type=jnp.float32,
    )
    carried = mixed
    return (new_highest, totals, carried)


def shards(
    latent,
    context,
    cond_latent,
    cond_context,
    mod_weight,
    w_query,
    w_key,
    w_value,
    w_out,
    head_lambda,
):
    width = latent.shape[1]
    heads = head_lambda.shape[0]
    conditioned = jax.nn.silu(jnp.stack([cond_latent, cond_context])).astype(jnp.bfloat16)
    partial_mod = jnp.dot(conditioned, mod_weight, preferred_element_type=jnp.float32)
    summed = lax.psum(partial_mod, "sp")
    modulation = lax.all_gather(summed, "tp", axis=1, tiled=True)
    shift_context = modulation[1, :width]
    scale_context = modulation[1, width : 2 * width]
    gate_latent = modulation[0, 2 * width :]
    own_rows = modulate_rows(latent, modulation[0, :width], modulation[0, width : 2 * width])
    group_rows = latent.shape[0] * lax.axis_size("tp")
    offset = lax.axis_index("sp") * group_rows
    piece = lax.all_gather(own_rows, "tp", axis=0, tiled=True)
    positions = offset + jnp.arange(piece.shape[0], dtype=jnp.int32)
    cosine, sine = rotary_tables(positions)
    query_part = rotate(jnp.dot(piece, w_query, preferred_element_type=jnp.float32), cosine, sine)
    key_part = rotate(jnp.dot(piece, w_key, preferred_element_type=jnp.float32), cosine, sine)
    value_part = jnp.dot(piece, w_value, preferred_element_type=jnp.float32).astype(jnp.bfloat16)
    projected = jnp.concatenate([query_part, key_part, value_part], axis=1)
    key_columns = heads * 2 * QK_DIM
    queries = projected[:, :key_columns].reshape(group_rows, heads, 2, QK_DIM)
    keys = projected[:, key_columns : 2 * key_columns]
    values = projected[:, 2 * key_columns :]
    initial = (
        jnp.full((heads, 2, group_rows), -1e30, jnp.float32),
        jnp.zeros((heads, 2, group_rows), jnp.float32),
        jnp.zeros((heads, 2, group_rows, VAL_DIM), jnp.float32),
    )
    own_context = modulate_rows(context, shift_context, scale_context)
    context_keys = jnp.dot(own_context, w_key, preferred_element_type=jnp.float32).astype(
        jnp.bfloat16
    )
    context_values = jnp.dot(own_context, w_value, preferred_element_type=jnp.float32).astype(
        jnp.bfloat16
    )
    joined_keys = jnp.concatenate([keys, context_keys], axis=0)
    joined_values = jnp.concatenate([values, context_values], axis=0)
    state = attend_piece(
        initial,
        (
            lax.all_gather(joined_keys, "sp", axis=0, tiled=True),
            lax.all_gather(joined_values, "sp", axis=0, tiled=True),
        ),
        queries,
    )
    highest, totals, carried = state
    factor = head_lambda[:, None, None]
    head_out = (
        carried[:, 0] / totals[:, 0][..., None] - factor * carried[:, 1] / totals[:, 1][..., None]
    )
    head_out = head_out * lax.rsqrt(
        jnp.mean(head_out * head_out, axis=-1, keepdims=True) + HEAD_EPS
    )
    attended = (
        jnp.transpose(head_out, (1, 0, 2)).reshape(group_rows, heads * VAL_DIM).astype(jnp.bfloat16)
    )
    branch = lax.psum_scatter(
        jnp.dot(attended, w_out, preferred_element_type=jnp.float32),
        "tp",
        scatter_dimension=0,
        tiled=True,
    )
    branch = branch * lax.rsqrt(jnp.mean(branch * branch, axis=-1, keepdims=True) + NORM_EPS)
    return (latent.astype(jnp.float32) + gate_latent * branch).astype(jnp.bfloat16)


def solution(mesh):
    placed = (
        P(("sp", "tp"), None),
        P("sp", None),
        P("sp"),
        P("sp"),
        P("sp", "tp"),
        P(None, "tp"),
        P(None, "tp"),
        P(None, "tp"),
        P("tp", None),
        P("tp"),
    )
    return jax.shard_map(
        shards, mesh=mesh, in_specs=placed, out_specs=P(("sp", "tp"), None), check_vma=False
    )
```

profile of v0, /device:TPU:8, one launch (start us, length us, event | category | flops | bytes accessed | tf_op | source)
XLA Modules:
  0.0 153.3 jit_solution(12564381263375404381)
XLA Ops:
  0.0 0.0 copy-start
  0.0 1.1 fusion.14
  1.1 0.0 copy-start.2
  1.2 0.0 copy-start.3
  1.2 1.5 fusion.6
  2.6 0.0 copy-done
  2.7 0.9 fusion.37
  3.6 7.0 %psum.7 = f32[2,768]{1,0:T(2,128)S(1)} all-reduce(f32[2,768]{1,0:T(2,128)S(1)} %fusion.37), channel_id=1, replica_groups=mesh['sp'=4,'tp'=8] {'sp'}, use_global_device_ids=true, to_apply=%region_0.1 | all-reduce | flops 1536 | bytes 12288 | tf_op jit(solution)/shard_map/psum | solution.py:90
  10.6 28.2 %all_gather.12 = f32[2,6144]{1,0:T(2,128)S(1)} all-gather(f32[2,768]{1,0:T(2,128)S(1)} %psum.7), channel_id=1, replica_groups=mesh['sp'=4,'tp'=8] {'tp'}, dimensions={1}, use_global_device_ids=true | all-gather | bytes 55296 | tf_op jit(solution)/shard_map/all_gather | solution.py:91
  38.9 0.0 copy-start.1
  38.9 1.8 %convolution_convert_fusion.1 = bf16[192,128]{1,0:T(8,128)(2,1)S(1)} fusion(bf16[2048,128]{1,0:T(8,128)(2,1)} %param.17, bf16[192,2048]{1,0:T(8,128)(2,1)} %param.11, f32[2048]{0:T(1024)S(1)} %bitcast.84, f32[2048]{0:T(1024)S(1)} %bitcast.86, f32[192]{0:T(256)S(1)} %add_rsqrt_fusion.1), kind=kOutput, calls=%fused_computation.14 | convolution fusion | flops 102653952 | bytes 1377024 | tf_op jit(solution)/shard_map/dot_general | solution.py:118
  40.7 0.0 copy-done.2
  40.7 0.0 copy-done.3
  40.7 0.5 convolution_convert_fusion.2
  41.2 0.0 copy-done.1
  41.2 0.1 fusion.19
  41.3 33.0 %all-gather = bf16[8,30,2048]{2,1,0:T(8,128)(2,1)S(1)} all-gather(bf16[1,30,2048]{2,1,0:T(8,128)(2,1)S(1)} %fusion.19), channel_id=1, replica_groups=mesh['sp'=4,'tp'=8] {'tp'}, dimensions={0}, use_global_device_ids=true | all-gather | bytes 1105920 | tf_op jit(solution)/shard_map/all_gather | solution.py:98
  74.3 0.3 reshape.355
  74.6 0.0 copy-start.4
  74.6 1.5 convolution_convert_fusion
  76.1 1.4 fusion.49
  78.2 0.1 broadcast_multiply_fusion.1
  78.3 0.1 fusion.35
  78.4 0.1 copy.21
  78.5 0.0 copy-done.4
  78.5 0.4 fusion.48
  78.9 0.1 copy.22
  79.0 0.1 copy.26
  79.2 0.1 copy.27
  79.3 0.1 copy.23
  79.5 0.1 copy.24
  79.6 6.3 %all_gather.14 = bf16[1728,128]{1,0:T(8,128)(2,1)S(1)} all-gather(bf16[432,128]{1,0:T(8,128)(2,1)S(1)} %pad_maximum_fusion), channel_id=1, replica_groups=mesh['sp'=4,'tp'=8] {'sp'}, dimensions={0}, use_global_device_ids=true | all-gather | bytes 552960 | tf_op jit(solution)/shard_map/all_gather | solution.py:126
  85.9 0.2 copy.28
  86.1 6.8 %all_gather.15 = bf16[1728,128]{1,0:T(8,128)(2,1)S(1)} all-gather(bf16[432,128]{1,0:T(8,128)(2,1)S(1)} %pad_maximum_fusion.1), channel_id=1, replica_groups=mesh['sp'=4,'tp'=8] {'sp'}, dimensions={0}, use_global_device_ids=true | all-gather | bytes 552960 | tf_op jit(solution)/shard_map/all_gather | solution.py:127
  92.9 0.7 fusion.47
  93.7 0.6 fusion.1
  94.3 0.0 copy-start.5
  94.3 0.7 fusion.10
  95.0 0.2 fusion.27
  95.2 0.1 copy-done.5
  95.3 0.0 copy-start.6
  95.3 0.5 fusion.28
  95.8 48.5 %fusion = f32[32,2048]{1,0:T(8,128)S(1)} fusion(f32[240,2048]{1,0:T(8,128)S(1)} %fusion.28), kind=kCustom, calls=%all-reduce-scatter | all-reduce-scatter fusion | flops 524289 | bytes 2228736
  144.3 4.3 %collective-permute-start = (f32[14,2048]{1,0:T(8,128)S(1)}, f32[14,2048]{1,0:T(8,128)S(1)}, u32[]{:S(2)}, u32[]{:S(2)}) collective-permute-start(f32[14,2048]{1,0:T(8,128)S(1)} %slice.97), channel_id=1, source_target_pairs={{0,1},{1,2},{2,3},{3,4},{4,5},{5,6},{6,7},{8,9},{9,10},{10,11},{11... | collective-permute-start | bytes 344072
  148.6 0.0 copy-done.6
  148.6 0.6 dynamic-slice.4
  149.9 2.2 %collective-permute-done = f32[14,2048]{1,0:T(8,128)S(1)} collective-permute-done((f32[14,2048]{1,0:T(8,128)S(1)}, f32[14,2048]{1,0:T(8,128)S(1)}, u32[]{:S(2)}, u32[]{:S(2)}) %collective-permute-start) | collective-permute-done | bytes 114720
  152.1 0.2 concatenate.28
  152.4 0.2 multiply_reduce_fusion
  152.5 0.8 fusion.18
  (16 shorter events, 0.2 us)
Async XLA Ops:
  0.0 2.6 %copy-start = (bf16[512,768]{1,0:T(8,128)(2,1)S(1)}, bf16[512,768]{1,0:T(8,128)(2,1)}, u32[]{:S(2)}) copy-start(bf16[512,768]{1,0:T(8,128)(2,1)} %param.14) | copy-start | bytes 2359300
  1.1 39.6 %copy-start.2 = (bf16[192,2048]{1,0:T(8,128)(2,1)S(1)}, bf16[192,2048]{1,0:T(8,128)(2,1)}, u32[]{:S(2)}) copy-start(bf16[192,2048]{1,0:T(8,128)(2,1)} %param.11) | copy-start | bytes 2359300
  1.2 39.5 %copy-start.3 = (bf16[2048,128]{1,0:T(8,128)(2,1)S(1)}, bf16[2048,128]{1,0:T(8,128)(2,1)}, u32[]{:S(2)}) copy-start(bf16[2048,128]{1,0:T(8,128)(2,1)} %param.16) | copy-start | bytes 1572868
  38.9 2.3 %copy-start.1 = (bf16[30,2048]{1,0:T(8,128)(2,1)S(1)}, bf16[30,2048]{1,0:T(8,128)(2,1)}, u32[]{:S(2)}) copy-start(bf16[30,2048]{1,0:T(8,128)(2,1)} %param.10) | copy-start | bytes 368644
  74.6 4.0 %copy-start.4 = (bf16[2048,128]{1,0:T(8,128)(2,1)S(1)}, bf16[2048,128]{1,0:T(8,128)(2,1)}, u32[]{:S(2)}) copy-start(bf16[2048,128]{1,0:T(8,128)(2,1)} %param.15) | copy-start | bytes 1572868
  94.3 1.0 copy-start.5
  95.3 53.3 %copy-start.6 = (u32[32]{0:T(128)S(1)}, u32[32]{0:T(128)}, u32[]{:S(2)}) copy-start(u32[32]{0:T(128)} %constant.70) | copy-start | bytes 388
  144.3 7.8 %collective-permute-start = (f32[14,2048]{1,0:T(8,128)S(1)}, f32[14,2048]{1,0:T(8,128)S(1)}, u32[]{:S(2)}, u32[]{:S(2)}) collective-permute-start(f32[14,2048]{1,0:T(8,128)S(1)} %slice.97), channel_id=1, source_target_pairs={{0,1},{1,2},{2,3},{3,4},{4,5},{5,6},{6,7},{8,9},{9,10},{10,11},{11... | collective-permute-start | bytes 344072
where the time goes:
time: 154 us; the launch traced here: 153 us
  blocking collectives  130 us (84%)
  matrix products  8.4 us (5%)
  other arithmetic  4.88 us (3%)
  starting transfers between devices  4.27 us (3%)
  waiting for transfers between devices  2.24 us (1%)
  local copies, waits for them, and re-layouts  2.05 us (1%)
  between operations  1.61 us (1%)
    unnamed x1, blocking collectives  48.5 us
    all_gather x1, blocking collectives, shards(): piece = lax.all_gather(own_rows, 'tp', axis=0, tiled=True)  33 us
    all_gather x1, blocking collectives, shards(): modulation = lax.all_gather(summed, 'tp', axis=1, tiled=True)  28.2 us
    psum x1, blocking collectives, shards(): summed = lax.psum(partial_mod, 'sp')  7.04 us
    all_gather x1, blocking collectives, shards(): lax.all_gather(joined_values, 'sp', axis=0, tiled=True)  6.83 us
    all_gather x1, blocking collectives, shards(): lax.all_gather(joined_keys, 'sp', axis=0, tiled=True)  6.28 us
    unnamed x1, starting transfers between devices  4.27 us
  transfers between devices with their start and end apart: 1, of which 1 were waited for; matrix products, arithmetic and copies ran while one was open for 0% of the time, Pallas kernels for 0%

commit v1 on v0

--- a/solution.py
+++ b/solution.py
@@ -9,6 +9,19 @@
 NORM_EPS = 0.01
 HEAD_EPS = 0.001
 THETA = 10000.0
+
+
+def name_sums_all(here_x):
+    along_axis = "tp"
+    sides = jax.lax.axis_size(along_axis)
+    gallery = [(nth, (nth + 1) % sides) for nth in range(sides)]
+    now = [None] * sides
+    now[sides - 1] = here_x
+    for i in range(sides - 2, -1, -1):
+        now[i] = jax.lax.ppermute(now[i + 1], axis_name=along_axis, perm=gallery)
+    found_now = jnp.concatenate(now, axis=1)
+    high = (jax.lax.axis_index(along_axis) + 1) * here_x.shape[1]
+    return jnp.roll(found_now, high, axis=1)
 
 
 def modulate_rows(rows, shift, scale):
@@ -88,7 +101,7 @@
     conditioned = jax.nn.silu(jnp.stack([cond_latent, cond_context])).astype(jnp.bfloat16)
     partial_mod = jnp.dot(conditioned, mod_weight, preferred_element_type=jnp.float32)
     summed = lax.psum(partial_mod, "sp")
-    modulation = lax.all_gather(summed, "tp", axis=1, tiled=True)
+    modulation = name_sums_all(summed)
     shift_context = modulation[1, :width]
     scale_context = modulation[1, width : 2 * width]
     gate_latent = modulation[0, 2 * width :]

time: 154 us -> 161 us (1.045)
  waiting for transfers between devices: 2.24 us -> 35.1 us
  blocking collectives: 130 us -> 102 us
    ppermute x0 -> x7, waiting for transfers between devices: none -> 31.2 us  [name_sums_all(): now[i] = jax.lax.ppermute(now[i + 1], axis_name=along_axis, perm=gallery)]
    all_gather x1 -> x0, blocking collectives: 28.2 us -> none  [shards(): modulation = lax.all_gather(summed, 'tp', axis=1, tiled=True)]
    all_gather x1, blocking collectives: 33 us -> 37.8 us  [shards(): piece = lax.all_gather(own_rows, 'tp', axis=0, tiled=True)]
    unnamed x1, blocking collectives: 48.5 us -> 44.5 us
    ppermute x0 -> x7, starting transfers between devices: none -> 2.18 us  [name_sums_all(): now[i] = jax.lax.ppermute(now[i + 1], axis_name=along_axis, perm=gallery)]
    unnamed x1, waiting for transfers between devices: 2.24 us -> 3.95 us
  transfers between devices with their start and end apart: 1 -> 8, of which waited for: 1 -> 8; matrix products, arithmetic and copies ran while one was open for 0% -> 2% of each run, Pallas kernels for 0% -> 0%
where the time goes in v1:
time: 161 us; the launch traced here: 160 us
  blocking collectives  102 us (63%)
  waiting for transfers between devices  35.1 us (22%)
  matrix products  7.09 us (4%)
  starting transfers between devices  5.81 us (4%)
  other arithmetic  4.83 us (3%)
  local copies, waits for them, and re-layouts  3.3 us (2%)
  between operations  1.67 us (1%)
    unnamed x1, blocking collectives  44.5 us
    all_gather x1, blocking collectives, shards(): piece = lax.all_gather(own_rows, 'tp', axis=0, tiled=True)  37.8 us
    ppermute x7, waiting for transfers between devices, name_sums_all(): now[i] = jax.lax.ppermute(now[i + 1], axis_name=along_axis, perm=gallery)  31.2 us
    psum x1, blocking collectives, shards(): summed = lax.psum(partial_mod, 'sp')  7.04 us
    all_gather x1, blocking collectives, shards(): lax.all_gather(joined_values, 'sp', axis=0, tiled=True)  6.83 us
    all_gather x1, blocking collectives, shards(): lax.all_gather(joined_keys, 'sp', axis=0, tiled=True)  6.28 us
    unnamed x1, waiting for transfers between devices  3.95 us
    unnamed x1, starting transfers between devices  3.62 us
  transfers between devices with their start and end apart: 8, of which 8 were waited for; matrix products, arithmetic and copies ran while one was open for 2% of the time, Pallas kernels for 0%

profile of v1, /device:TPU:8, one launch (start us, length us, event | category | flops | bytes accessed | tf_op | source)
XLA Modules:
  0.0 160.2 jit_solution(11692758033670076608)
XLA Ops:
  0.0 0.0 copy-start
  0.0 0.0 copy-start.2
  0.0 0.0 copy-start.3
  0.0 1.1 copy-done
  1.1 0.9 fusion.37
  2.0 7.0 %psum.7 = f32[2,768]{1,0:T(2,128)S(1)} all-reduce(f32[2,768]{1,0:T(2,128)S(1)} %fusion.37), channel_id=1, replica_groups=mesh['sp'=4,'tp'=8] {'sp'}, use_global_device_ids=true, to_apply=%region_0.1 | all-reduce | flops 1536 | bytes 12288 | tf_op jit(solution)/shard_map/psum | solution.py:103
  9.1 1.5 collective-permute-start
  10.7 3.0 %collective-permute-done = f32[2,768]{1,0:T(2,128)S(1)} collective-permute-done((f32[2,768]{1,0:T(2,128)S(1)}, f32[2,768]{1,0:T(2,128)S(1)}, u32[]{:S(2)}, u32[]{:S(2)}) %collective-permute-start) | collective-permute-done | bytes 6176 | tf_op jit(solution)/shard_map/ppermute | solution.py:21
  13.7 0.6 collective-permute-start.1
  14.3 0.1 broadcast_multiply_fusion.1
  14.4 0.0 copy-start.4
  14.4 3.8 %collective-permute-done.1 = f32[2,768]{1,0:T(2,128)S(1)} collective-permute-done((f32[2,768]{1,0:T(2,128)S(1)}, f32[2,768]{1,0:T(2,128)S(1)}, u32[]{:S(2)}, u32[]{:S(2)}) %collective-permute-start.1) | collective-permute-done | bytes 6176 | tf_op jit(solution)/shard_map/ppermute | solution.py:21
  18.2 0.0 collective-permute-start.2
  18.2 1.4 fusion.6
  19.6 3.2 %collective-permute-done.2 = f32[2,768]{1,0:T(2,128)S(1)} collective-permute-done((f32[2,768]{1,0:T(2,128)S(1)}, f32[2,768]{1,0:T(2,128)S(1)}, u32[]{:S(2)}, u32[]{:S(2)}) %collective-permute-start.2) | collective-permute-done | bytes 6176 | tf_op jit(solution)/shard_map/ppermute | solution.py:21
  22.7 0.0 collective-permute-start.3
  22.7 4.5 %collective-permute-done.3 = f32[2,768]{1,0:T(2,128)S(1)} collective-permute-done((f32[2,768]{1,0:T(2,128)S(1)}, f32[2,768]{1,0:T(2,128)S(1)}, u32[]{:S(2)}, u32[]{:S(2)}) %collective-permute-start.3) | collective-permute-done | bytes 6176 | tf_op jit(solution)/shard_map/ppermute | solution.py:21
  27.3 0.0 collective-permute-start.4
  27.3 1.0 fusion.14
  28.3 4.9 %collective-permute-done.4 = f32[2,768]{1,0:T(2,128)S(1)} collective-permute-done((f32[2,768]{1,0:T(2,128)S(1)}, f32[2,768]{1,0:T(2,128)S(1)}, u32[]{:S(2)}, u32[]{:S(2)}) %collective-permute-start.4) | collective-permute-done | bytes 6176 | tf_op jit(solution)/shard_map/ppermute | solution.py:21
  33.3 0.0 collective-permute-start.5
  33.3 6.3 %collective-permute-done.5 = f32[2,768]{1,0:T(2,128)S(1)} collective-permute-done((f32[2,768]{1,0:T(2,128)S(1)}, f32[2,768]{1,0:T(2,128)S(1)}, u32[]{:S(2)}, u32[]{:S(2)}) %collective-permute-start.5) | collective-permute-done | bytes 6176 | tf_op jit(solution)/shard_map/ppermute | solution.py:21
  39.6 0.0 collective-permute-start.6
  39.6 0.1 fusion.35
  40.4 0.1 copy.21
  40.5 5.4 %collective-permute-done.6 = f32[2,768]{1,0:T(2,128)S(1)} collective-permute-done((f32[2,768]{1,0:T(2,128)S(1)}, f32[2,768]{1,0:T(2,128)S(1)}, u32[]{:S(2)}, u32[]{:S(2)}) %collective-permute-start.6) | collective-permute-done | bytes 6176 | tf_op jit(solution)/shard_map/ppermute | solution.py:21
  46.1 0.2 constant_dynamic-slice_fusion.1
  46.2 0.0 copy-done.2
  46.3 0.0 copy-done.3
  46.3 0.0 copy-start.1
  46.3 0.5 convolution_convert_fusion.1
  46.7 0.0 copy-done.4
  46.8 0.5 convolution_convert_fusion.2
  47.2 0.0 copy-done.1
  47.2 0.1 fusion.19
  47.3 37.8 %all-gather = bf16[8,30,2048]{2,1,0:T(8,128)(2,1)S(1)} all-gather(bf16[1,30,2048]{2,1,0:T(8,128)(2,1)S(1)} %fusion.19), channel_id=1, replica_groups=mesh['sp'=4,'tp'=8] {'tp'}, dimensions={0}, use_global_device_ids=true | all-gather | bytes 1105920 | tf_op jit(solution)/shard_map/all_gather | solution.py:111
  85.1 0.3 reshape.355
  85.4 0.0 copy-start.5
  85.4 1.5 convolution_convert_fusion
  86.9 1.4 fusion.48
  88.4 0.0 copy-done.5
  88.4 0.4 fusion.47
  88.8 0.1 copy.22
  88.9 0.1 copy.26
  89.0 0.1 copy.27
  89.1 0.1 copy.23
  89.3 0.1 copy.24
  89.4 6.3 %all_gather.10 = bf16[1728,128]{1,0:T(8,128)(2,1)S(1)} all-gather(bf16[432,128]{1,0:T(8,128)(2,1)S(1)} %pad_maximum_fusion), channel_id=1, replica_groups=mesh['sp'=4,'tp'=8] {'sp'}, dimensions={0}, use_global_device_ids=true | all-gather | bytes 552960 | tf_op jit(solution)/shard_map/all_gather | solution.py:139
  95.7 0.2 copy.28
  95.9 6.8 %all_gather.11 = bf16[1728,128]{1,0:T(8,128)(2,1)S(1)} all-gather(bf16[432,128]{1,0:T(8,128)(2,1)S(1)} %pad_maximum_fusion.1), channel_id=1, replica_groups=mesh['sp'=4,'tp'=8] {'sp'}, dimensions={0}, use_global_device_ids=true | all-gather | bytes 552960 | tf_op jit(solution)/shard_map/all_gather | solution.py:140
  102.8 0.7 fusion.46
  103.5 0.6 fusion.1
  104.1 0.7 fusion.10
  104.8 0.2 fusion.27
  105.1 0.1 copy-done.6
  105.2 0.5 fusion.28
  105.7 44.5 %fusion = f32[32,2048]{1,0:T(8,128)S(1)} fusion(f32[240,2048]{1,0:T(8,128)S(1)} %fusion.28), kind=kCustom, calls=%all-reduce-scatter | all-reduce-scatter fusion | flops 524289 | bytes 2228736
  150.2 3.6 %collective-permute-start.7 = (f32[14,2048]{1,0:T(8,128)S(1)}, f32[14,2048]{1,0:T(8,128)S(1)}, u32[]{:S(2)}, u32[]{:S(2)}) collective-permute-start(f32[14,2048]{1,0:T(8,128)S(1)} %slice.92), channel_id=1, source_target_pairs={{0,1},{1,2},{2,3},{3,4},{4,5},{5,6},{6,7},{8,9},{9,10},{10,11},{11... | collective-permute-start | bytes 344072
  153.8 0.0 copy-done.7
  153.8 0.6 dynamic-slice.9
  155.1 4.0 %collective-permute-done.7 = f32[14,2048]{1,0:T(8,128)S(1)} collective-permute-done((f32[14,2048]{1,0:T(8,128)S(1)}, f32[14,2048]{1,0:T(8,128)S(1)}, u32[]{:S(2)}, u32[]{:S(2)}) %collective-permute-start.7) | collective-permute-done | bytes 114720
  159.0 0.2 concatenate.35
  159.3 0.2 multiply_reduce_fusion
  159.4 0.8 fusion.18
  (33 shorter events, 0.3 us)
Async XLA Ops:
  0.0 1.1 copy-start
  0.0 46.2 %copy-start.2 = (bf16[192,2048]{1,0:T(8,128)(2,1)S(1)}, bf16[192,2048]{1,0:T(8,128)(2,1)}, u32[]{:S(2)}) copy-start(bf16[192,2048]{1,0:T(8,128)(2,1)} %param.11) | copy-start | bytes 2359300
  0.0 46.3 %copy-start.3 = (bf16[2048,128]{1,0:T(8,128)(2,1)S(1)}, bf16[2048,128]{1,0:T(8,128)(2,1)}, u32[]{:S(2)}) copy-start(bf16[2048,128]{1,0:T(8,128)(2,1)} %param.17) | copy-start | bytes 1572868
  9.1 4.6 %collective-permute-start = (f32[2,768]{1,0:T(2,128)S(1)}, f32[2,768]{1,0:T(2,128)S(1)}, u32[]{:S(2)}, u32[]{:S(2)}) collective-permute-start(f32[2,768]{1,0:T(2,128)S(1)} %psum.7), channel_id=1, source_target_pairs={{0,1},{1,2},{2,3},{3,4},{4,5},{5,6},{6,7},{7,0},{8,9},{9,10},{10,1... | collective-permute-start | bytes 18440 | tf_op jit(solution)/shard_map/ppermute | solution.py:21
  13.7 4.5 %collective-permute-start.1 = (f32[2,768]{1,0:T(2,128)S(1)}, f32[2,768]{1,0:T(2,128)S(1)}, u32[]{:S(2)}, u32[]{:S(2)}) collective-permute-start(f32[2,768]{1,0:T(2,128)S(1)} %collective-permute-done), channel_id=1, source_target_pairs={{0,1},{1,2},{2,3},{3,4},{4,5},{5,6},{6,7},{7,0},{8,9},{9,10},{10,1... | collective-permute-start | bytes 18440 | tf_op jit(solution)/shard_map/ppermute | solution.py:21
  14.4 32.4 %copy-start.4 = (bf16[2048,128]{1,0:T(8,128)(2,1)S(1)}, bf16[2048,128]{1,0:T(8,128)(2,1)}, u32[]{:S(2)}) copy-start(bf16[2048,128]{1,0:T(8,128)(2,1)} %param.16) | copy-start | bytes 1572868
  18.2 4.5 %collective-permute-start.2 = (f32[2,768]{1,0:T(2,128)S(1)}, f32[2,768]{1,0:T(2,128)S(1)}, u32[]{:S(2)}, u32[]{:S(2)}) collective-permute-start(f32[2,768]{1,0:T(2,128)S(1)} %collective-permute-done.1), channel_id=1, source_target_pairs={{0,1},{1,2},{2,3},{3,4},{4,5},{5,6},{6,7},{7,0},{8,9},{9,10},{10,1... | collective-permute-start | bytes 18440 | tf_op jit(solution)/shard_map/ppermute | solution.py:21
  22.7 4.5 %collective-permute-start.3 = (f32[2,768]{1,0:T(2,128)S(1)}, f32[2,768]{1,0:T(2,128)S(1)}, u32[]{:S(2)}, u32[]{:S(2)}) collective-permute-start(f32[2,768]{1,0:T(2,128)S(1)} %collective-permute-done.2), channel_id=1, source_target_pairs={{0,1},{1,2},{2,3},{3,4},{4,5},{5,6},{6,7},{7,0},{8,9},{9,10},{10,1... | collective-permute-start | bytes 18440 | tf_op jit(solution)/shard_map/ppermute | solution.py:21
  27.3 6.0 %collective-permute-start.4 = (f32[2,768]{1,0:T(2,128)S(1)}, f32[2,768]{1,0:T(2,128)S(1)}, u32[]{:S(2)}, u32[]{:S(2)}) collective-permute-start(f32[2,768]{1,0:T(2,128)S(1)} %collective-permute-done.3), channel_id=1, source_target_pairs={{0,1},{1,2},{2,3},{3,4},{4,5},{5,6},{6,7},{7,0},{8,9},{9,10},{10,1... | collective-permute-start | bytes 18440 | tf_op jit(solution)/shard_map/ppermute | solution.py:21
  33.3 6.3 %collective-permute-start.5 = (f32[2,768]{1,0:T(2,128)S(1)}, f32[2,768]{1,0:T(2,128)S(1)}, u32[]{:S(2)}, u32[]{:S(2)}) collective-permute-start(f32[2,768]{1,0:T(2,128)S(1)} %collective-permute-done.4), channel_id=1, source_target_pairs={{0,1},{1,2},{2,3},{3,4},{4,5},{5,6},{6,7},{7,0},{8,9},{9,10},{10,1... | collective-permute-start | bytes 18440 | tf_op jit(solution)/shard_map/ppermute | solution.py:21
  39.6 6.3 %collective-permute-start.6 = (f32[2,768]{1,0:T(2,128)S(1)}, f32[2,768]{1,0:T(2,128)S(1)}, u32[]{:S(2)}, u32[]{:S(2)}) collective-permute-start(f32[2,768]{1,0:T(2,128)S(1)} %collective-permute-done.5), channel_id=1, source_target_pairs={{0,1},{1,2},{2,3},{3,4},{4,5},{5,6},{6,7},{7,0},{8,9},{9,10},{10,1... | collective-permute-start | bytes 18440 | tf_op jit(solution)/shard_map/ppermute | solution.py:21
  46.3 0.9 copy-start.1
  85.4 3.0 %copy-start.5 = (bf16[2048,128]{1,0:T(8,128)(2,1)S(1)}, bf16[2048,128]{1,0:T(8,128)(2,1)}, u32[]{:S(2)}) copy-start(bf16[2048,128]{1,0:T(8,128)(2,1)} %param.15) | copy-start | bytes 1572868
  104.1 1.0 copy-start.6
  105.2 48.6 %copy-start.7 = (u32[32]{0:T(128)S(1)}, u32[32]{0:T(128)}, u32[]{:S(2)}) copy-start(u32[32]{0:T(128)} %constant.94) | copy-start | bytes 388
  150.2 8.8 %collective-permute-start.7 = (f32[14,2048]{1,0:T(8,128)S(1)}, f32[14,2048]{1,0:T(8,128)S(1)}, u32[]{:S(2)}, u32[]{:S(2)}) collective-permute-start(f32[14,2048]{1,0:T(8,128)S(1)} %slice.92), channel_id=1, source_target_pairs={{0,1},{1,2},{2,3},{3,4},{4,5},{5,6},{6,7},{8,9},{9,10},{10,11},{11... | collective-permute-start | bytes 344072
